TPU v7x, 32 devices: a whole 2x2x4 slice. The times are simulated.
32 devices in a mesh: grp: 2 (over y), dp: 2 (over x), kv: 4 (over z), tp: 2 (over core).
Axes of the slice: x: 2, y: 2, z: 4, core: 2. Of those that a mesh axis runs over, the one named last changes fastest.
Arguments:
- tokens: bfloat16 [32, 2048], P(('grp', 'dp'), ('kv', 'tp')), parts along dimension 0, may hold values from -40 to 40
- past_state: float32 [32, 16, 128, 128], P(('grp', 'dp', 'kv'), 'tp'), parts along dimension 0, may hold values from -4 to 4
- mix_gain: float32 [2048], P('kv'), may hold values from 0.1 to 1.9
- w_query: bfloat16 [2048, 2048], P('kv', 'tp'), may hold values from -0.125 to 0.125
- w_forget: bfloat16 [2048, 2048], P('kv', 'tp'), may hold values from -0.125 to 0.125
- w_value: bfloat16 [2048, 2048], P('kv', 'tp'), may hold values from -0.125 to 0.125
- w_gate_out: bfloat16 [2048, 2048], P('kv', 'tp'), may hold values from -0.125 to 0.125
- floor_logits: float32 [2048], P('tp'), may hold values from -6 to 6
- head_gain: float32 [128], replicated, may hold values from 0.1 to 1.9
- w_out: bfloat16 [2048, 2048], P(None, ('kv', 'tp')), may hold values from -0.125 to 0.125
- mlp_gain: float32 [2048], replicated, may hold values from 0.1 to 1.9
- w_gate: bfloat16 [2048, 5632], P(None, ('kv', 'tp')), may hold values from -0.125 to 0.125
- w_up: bfloat16 [2048, 5632], P(None, ('kv', 'tp')), may hold values from -0.125 to 0.125
- w_down: bfloat16 [5632, 2048], P(('kv', 'tp')), may hold values from -0.109375 to 0.109375
Outputs:
- result: bfloat16 [32, 2048], P(('grp', 'dp'), ('kv', 'tp')), parts along dimension 0
- new_state: float32 [32, 16, 128, 128], P(('grp', 'dp', 'kv'), 'tp'), parts along dimension 0
There are 2 independent parts, one for each index of `grp`. A program takes and returns all parts, laid end to end along the dimension named above; an argument that names none is the same for every part. Nothing has to cross between parts.
All inputs are finite; a program needn't handle non-finite values.
Results may differ from a plain program's by a relative error of at most 0.0091.
Values may be sent and summed in bfloat16 or wider, within the bound.
A program may use at most 64 MiB of HBM per device.

v0:
```python
import jax
import jax.numpy as jnp
from jax import lax
from jax.sharding import PartitionSpec as P

D = 2048
DK = 128
DV = 128
epsilon = 1e-06


def body(
    tokens,
    past_state,
    mix_gain,
    w_query,
    w_forget,
    w_value,
    w_gate_out,
    floor_logits,
    head_gain,
    w_out,
    mlp_gain,
    w_gate,
    w_up,
    w_down,
):
    kv_count = lax.axis_size("kv")
    tp_count = lax.axis_size("tp")
    rows_local = past_state.shape[0]
    heads_local = past_state.shape[1]
    width_cols = tokens.shape[1]
    own_block = lax.all_gather(tokens, "tp", axis=1, tiled=True)
    block_f = own_block.astype(jnp.float32)
    square_rows = lax.psum(jnp.sum(block_f * block_f, axis=1), "kv")
    gained = (own_block.astype(jnp.float32) * mix_gain).astype(jnp.bfloat16)
    mine = lax.dynamic_slice_in_dim(square_rows, lax.axis_index("kv") * rows_local, rows_local, 0)
    row_scale = lax.rsqrt(mine / D + epsilon)[:, None]
    query_sum, forget_sum, value_sum, gate_sum = (
        lax.psum_scatter(
            jnp.dot(gained, w_query, preferred_element_type=jnp.float32),
            "kv",
            scatter_dimension=0,
            tiled=True,
        ),
        lax.psum_scatter(
            jnp.dot(gained, w_forget, preferred_element_type=jnp.float32),
            "kv",
            scatter_dimension=0,
            tiled=True,
        ),
        lax.psum_scatter(
            jnp.dot(gained, w_value, preferred_element_type=jnp.float32),
            "kv",
            scatter_dimension=0,
            tiled=True,
        ),
        lax.psum_scatter(
            jnp.dot(gained, w_gate_out, preferred_element_type=jnp.float32),
            "kv",
            scatter_dimension=0,
            tiled=True,
        ),
    )
    query = query_sum * row_scale
    forget_pre = forget_sum * row_scale
    value = value_sum * row_scale
    gate_pre = gate_sum * row_scale
    lower = jax.nn.sigmoid(floor_logits).reshape(heads_local, DK)
    forget = lower + (1.0 - lower) * jax.nn.sigmoid(forget_pre.reshape(rows_local, heads_local, DK))
    values = value.reshape(rows_local, heads_local, DV)
    new_state = forget[..., None] * past_state + (1.0 - forget)[..., None] * values[:, :, None, :]
    activ = jax.nn.silu(query.reshape(rows_local, heads_local, DK))
    head_out = jnp.einsum("shkv,shk->shv", new_state, activ, precision=lax.Precision.HIGHEST)
    normed = head_out * lax.rsqrt(jnp.mean(head_out * head_out, axis=2, keepdims=True) + epsilon)
    normed = normed * head_gain * jax.nn.silu(gate_pre.reshape(rows_local, heads_local, DV))
    mixed = normed.reshape(1, rows_local, heads_local * DV).astype(jnp.bfloat16)
    every_head = lax.all_gather(mixed, ("kv", "tp"), axis=0, tiled=True)
    every_head = every_head.reshape(kv_count, tp_count, rows_local, heads_local * DV)
    out_blocks = w_out.reshape(tp_count, heads_local * DV, width_cols)
    projected = jnp.einsum(
        "ktsh,thc->ksc", every_head, out_blocks, preferred_element_type=jnp.float32
    )
    middle = (
        tokens.astype(jnp.float32) + projected.reshape(kv_count * rows_local, width_cols)
    ).astype(jnp.bfloat16)
    gathered = lax.all_gather(middle, ("kv", "tp"), axis=1, tiled=True)
    gathered_f = gathered.astype(jnp.float32)
    mlp_scale = lax.rsqrt(jnp.mean(gathered_f * gathered_f, axis=1, keepdims=True) + epsilon)
    mlp_in = (gathered_f * mlp_scale * mlp_gain).astype(jnp.bfloat16)
    gate = jnp.dot(mlp_in, w_gate, preferred_element_type=jnp.float32)
    upward = jnp.dot(mlp_in, w_up, preferred_element_type=jnp.float32)
    hidden = (jax.nn.silu(gate) * upward).astype(jnp.bfloat16)
    terms = jnp.dot(hidden, w_down, preferred_element_type=jnp.float32)
    summed = lax.psum_scatter(terms, ("kv", "tp"), scatter_dimension=1, tiled=True)
    result = (middle.astype(jnp.float32) + summed).astype(jnp.bfloat16)
    return (result, new_state)


def solution(mesh):
    placed = (
        P(("grp", "dp"), ("kv", "tp")),
        P(("grp", "dp", "kv"), "tp", None, None),
        P("kv"),
        P("kv", "tp"),
        P("kv", "tp"),
        P("kv", "tp"),
        P("kv", "tp"),
        P("tp"),
        P(),
        P(None, ("kv", "tp")),
        P(),
        P(None, ("kv", "tp")),
        P(None, ("kv", "tp")),
        P(("kv", "tp"), None),
    )
    return jax.shard_map(
        body,
        mesh=mesh,
        in_specs=placed,
        out_specs=(P(("grp", "dp"), ("kv", "tp")), P(("grp", "dp", "kv"), "tp", None, None)),
        check_vma=False,
    )
```

profile of v0, /device:TPU:0, one launch (start us, length us, event | category | flops | bytes accessed | tf_op | source)
XLA Modules:
  0.0 136.3 jit_solution(9865820180472469167)
XLA Ops:
  7.3 2.2 %all_gather.9 = bf16[8,512]{1,0:T(8,128)(2,1)S(1)} all-gather(bf16[8,256]{1,0:T(8,128)(2,1)} %param.14), channel_id=1, replica_groups=mesh['grp'=2,'dp'=2,'kv'=4,'tp'=2] {'tp'}, dimensions={1}, use_global_device_ids=true | all-gather | bytes 12288 | tf_op jit(solution)/shard_map/all_gather | solution.py:33
  9.5 0.6 fusion.13
  10.1 2.1 %fusion.38 = f32[8,1024]{1,0:T(8,128)} fusion(bf16[512,1024]{1,0:T(8,128)(2,1)} %param.19, bf16[8,512]{1,0:T(8,128)(2,1)S(1)} %all_gather.9, f32[512]{0:T(512)} %param.16), kind=kOutput, calls=%fused_computation.55 | convolution fusion | flops 8400896 | bytes 1091584 | tf_op jit(solution)/shard_map/dot_general | solution.py:53
  12.2 2.1 %fusion.36 = f32[8,1024]{1,0:T(8,128)} fusion(bf16[512,1024]{1,0:T(8,128)(2,1)} %param.17, bf16[8,512]{1,0:T(8,128)(2,1)S(1)} %all_gather.9, f32[512]{0:T(512)} %param.16), kind=kOutput, calls=%fused_computation.54 | convolution fusion | flops 8400896 | bytes 1091584 | tf_op jit(solution)/shard_map/dot_general | solution.py:41
  14.3 2.1 %fusion.34 = f32[8,1024]{1,0:T(8,128)} fusion(bf16[512,1024]{1,0:T(8,128)(2,1)} %param.20, bf16[8,512]{1,0:T(8,128)(2,1)S(1)} %all_gather.9, f32[512]{0:T(512)} %param.16), kind=kOutput, calls=%fused_computation.53 | convolution fusion | flops 8400896 | bytes 1091584 | tf_op jit(solution)/shard_map/dot_general | solution.py:59
  16.5 0.9 fusion.40
  17.4 0.0 reduce-scatter.2.cloned.1.call-start
  17.5 0.7 dynamic-slice
  18.8 36.2 %all-reduce.7.cloned.1.call-done = (f32[8,1024]{1,0:T(8,128)}, f32[8]{0:T(128)}, f32[8,1024]{1,0:T(8,128)}, f32[8,1024]{1,0:T(8,128)}, f32[8,1024]{1,0:T(8,128)}) async-done(((f32[8,1024]{1,0:T(8,128)}, f32[8]{0:T(128)}, f32[8,1024]{1,0:T(8,128)}, f32[8,1024]{1,0:T(8,128)}, f32[8,1024]{1,0:T(8,128)}), (f32[8,1024]{1,0:T(8,128)}, f32[8]{0:T(128)}, f32[8,1024]{1,0:T(8,128)}, f32[8,1024]{1,0:T(8,128)}, ...) | async-done | bytes 131120
  55.1 0.8 add_rsqrt_fusion.2
  55.8 0.9 fusion.24
  56.8 1.8 %multiply_add_fusion = f32[2,8,128,128]{3,2,1,0:T(8,128)S(1)} fusion(f32[2,8,128,128]{3,2,1,0:T(8,128)} %param.15, f32[2,8,128]{2,1,0:T(8,128)S(1)} %bitcast.79, f32[2,8,128]{2,1,0:T(8,128)S(1)} %get-tuple-element.7, f32[2,8,128]{2,1,0:T(8,128)S(1)} %get-tuple-element.8), kind=kLoop, calls=%fused_computation.6 | loop fusion | flops 786432 | bytes 2121728 | tf_op jit(solution)/shard_map/add | solution.py:72
  58.6 1.0 copy-done.1
  59.6 1.0 fusion.44
  60.6 0.1 multiply_reduce_fusion
  60.7 0.1 fusion.29
  60.8 14.1 %all_gather.10 = bf16[8,2,1024]{2,1,0:T(2,128)(2,1)S(1)} all-gather(bf16[1,2,1024]{2,1,0:T(2,128)(2,1)S(1)} %convert_element_type.46), channel_id=1, replica_groups=mesh['grp'=2,'dp'=2,'kv'=4,'tp'=2] {'kv','tp'}, dimensions={0}, use_global_device_ids=true | all-gather | bytes 36864 | tf_op jit(solution)/shard_map/all_gather | solution.py:78
  74.9 1.5 %fusion.3 = bf16[8,256]{1,0:T(8,128)(2,1)S(1)} fusion(bf16[8,1024,2]{1,0,2:T(8,128)(2,1)S(1)} %dot_general.37, bf16[2,1024,256]{2,1,0:T(8,128)(2,1)} %bitcast.75, bf16[8,256]{1,0:T(8,128)(2,1)S(1)} %copy-done.5), kind=kOutput, calls=%fused_computation.5 | convolution fusion | flops 8394752 | bytes 1089536 | tf_op jit(solution)/shard_map/ktsh,thc->ksc/dot_general | solution.py:81
  76.4 14.1 %all_gather.11 = bf16[8,2048]{1,0:T(8,128)(2,1)S(1)} all-gather(bf16[8,256]{1,0:T(8,128)(2,1)S(1)} %fusion.3), channel_id=1, replica_groups=mesh['grp'=2,'dp'=2,'kv'=4,'tp'=2] {'kv','tp'}, dimensions={1}, use_global_device_ids=true | all-gather | bytes 36864 | tf_op jit(solution)/shard_map/all_gather | solution.py:87
  90.5 0.1 fusion.4
  90.6 2.7 %fusion.32 = f32[8,704]{1,0:T(8,128)S(1)} fusion(bf16[2048,704]{0,1:T(8,128)(2,1)} %param.25, bf16[8,2048]{1,0:T(8,128)(2,1)S(1)} %all_gather.11, f32[2048]{0:T(1024)S(1)} %copy-done.3, f32[8]{0:T(128)S(1)} %add_rsqrt_fusion.1), kind=kOutput, calls=%fused_computation.50 | convolution fusion | flops 23134208 | bytes 2947104 | tf_op jit(solution)/shard_map/dot_general | solution.py:91
  93.3 4.1 %fusion.1 = f32[8,2048]{1,0:T(8,128)} fusion(bf16[704,2048]{1,0:T(8,128)(2,1)S(1)} %copy-done, bf16[2048,704]{0,1:T(8,128)(2,1)} %param.26, f32[8,704]{1,0:T(8,128)S(1)} %fusion.32, bf16[8,2048]{1,0:T(8,128)(2,1)S(1)} %all_gather.11, f32[2048]{0:T(1024)S(1)} %copy-done.3, f32[8]{0:T(128)S(1)} %add_rsqrt_fusion.1), kind=kOutput, calls=%fused_computation.2 | convolution fusion | flops 46236672 | bytes 5896224 | tf_op jit(solution)/shard_map/dot_general | solution.py:94
  97.4 30.7 %reduce-scatter.2.cloned.1.call-done = f32[8,256]{1,0:T(8,128)} async-done(((f32[8,2048]{1,0:T(8,128)}), f32[8,256]{1,0:T(8,128)}) %reduce-scatter.2.cloned.1.call-update) | async-done | bytes 8208 | tf_op jit(solution)/shard_map/reduce_scatter | solution.py:95
  128.2 1.3 add_convert_fusion
  (29 shorter events, 0.2 us)
Async XLA Ops:
  7.2 86.1 %copy-start = (bf16[704,2048]{1,0:T(8,128)(2,1)S(1)}, bf16[704,2048]{1,0:T(8,128)(2,1)}, u32[]{:S(2)}) copy-start(bf16[704,2048]{1,0:T(8,128)(2,1)} %param.27) | copy-start | bytes 8650756
  7.2 10.3 %copy-start.8 = (u32[32]{0:T(128)S(1)}, u32[32]{0:T(128)}, u32[]{:S(2)}) copy-start(u32[32]{0:T(128)} %constant.38) | copy-start | bytes 388
  7.2 9.3 %copy-start.4 = (f32[512]{0:T(512)S(1)}, f32[512]{0:T(512)}, u32[]{:S(2)}) copy-start(f32[512]{0:T(512)} %param.16) | copy-start | bytes 6148
  7.2 10.2 %copy-start.6 = (f32[1024]{0:T(1024)S(1)}, f32[1024]{0:T(1024)}, u32[]{:S(2)}) copy-start(f32[1024]{0:T(1024)} %param.21) | copy-start | bytes 12292
  7.2 47.9 %all-reduce.7.cloned.1.call-start = ((), (), s32[]{:S(2)}) async-start(), calls=%async_computation.2 | async-start | bytes 263168
  7.3 9.2 %copy-start.2 = (bf16[512,1024]{1,0:T(8,128)(2,1)S(1)}, bf16[512,1024]{1,0:T(8,128)(2,1)}, u32[]{:S(2)}) copy-start(bf16[512,1024]{1,0:T(8,128)(2,1)} %param.18) | copy-start | bytes 3145732
  14.3 46.4 %copy-start.7 = (f32[128]{0:T(128)S(1)}, f32[128]{0:T(128)}, u32[]{:S(2)}) copy-start(f32[128]{0:T(128)} %param.22) | copy-start | bytes 1540
  14.3 60.6 %copy-start.5 = (bf16[8,256]{1,0:T(8,128)(2,1)S(1)}, bf16[8,256]{1,0:T(8,128)(2,1)}, u32[]{:S(2)}) copy-start(bf16[8,256]{1,0:T(8,128)(2,1)} %param.14) | copy-start | bytes 12292
  16.5 74.2 %copy-start.3 = (f32[2048]{0:T(1024)S(1)}, f32[2048]{0:T(1024)}, u32[]{:S(2)}) copy-start(f32[2048]{0:T(1024)} %param.24) | copy-start | bytes 24580
  17.4 110.8 %reduce-scatter.2.cloned.1.call-start = ((), (), s32[]{:S(2)}) async-start(), calls=%async_computation.1 | async-start | bytes 73728 | tf_op jit(solution)/shard_map/reduce_scatter | solution.py:95
  58.6 1.0 copy-start.1
Sparse Core Ops, SparseCore 0:
  17.5 37.5 all-reduce.6
  97.6 30.5 reduce-scatter.1
where the time goes:
time: 137 us; the launch traced here: 136 us
  waiting for transfers between devices  67 us (49%)
  blocking collectives  30.4 us (22%)
  matrix products  16.4 us (12%)
  between operations  14.9 us (11%)
  other arithmetic  5.75 us (4%)
  local copies, waits for them, and re-layouts  1.73 us (1%)
    unnamed x3, waiting for transfers between devices  36.3 us
    reduce_scatter x1, waiting for transfers between devices, body(): lax.psum_scatter(terms, ('kv', 'tp'), scatter_dimension=1, tiled=True)  30.7 us
    all_gather x1, blocking collectives, body(): every_head = lax.all_gather(mixed, ('kv', 'tp'), axis=0, tiled=True)  14.1 us
    all_gather x1, blocking collectives, body(): gathered = lax.all_gather(middle, ('kv', 'tp'), axis=1, tiled=True)  14.1 us
    dot_general x1, matrix products, body(): terms = jnp.dot(hidden, w_down, preferred_element_type=jnp.float32)  4.12 us
  transfers between devices with their start and end apart: 2, of which 2 were waited for; matrix products, arithmetic and copies ran while one was open for 0% of the time, Pallas kernels for 0%

commit v1 on v0

--- a/solution.py
+++ b/solution.py
@@ -84,7 +84,10 @@
     middle = (
         tokens.astype(jnp.float32) + projected.reshape(kv_count * rows_local, width_cols)
     ).astype(jnp.bfloat16)
-    gathered = lax.all_gather(middle, ("kv", "tp"), axis=1, tiled=True)
+    gathered = jnp.concatenate(
+        lax.all_to_all(jnp.stack([middle] * lax.axis_size(("kv", "tp"))), ("kv", "tp"), 0, 0),
+        axis=1,
+    )
     gathered_f = gathered.astype(jnp.float32)
     mlp_scale = lax.rsqrt(jnp.mean(gathered_f * gathered_f, axis=1, keepdims=True) + epsilon)
     mlp_in = (gathered_f * mlp_scale * mlp_gain).astype(jnp.bfloat16)

time: 137 us -> 130 us (0.949)
  blocking collectives: 30.4 us -> 25.6 us
  waiting for transfers between devices: 67 us -> 65.2 us
    all_gather x1 -> x0, blocking collectives: 14.1 us -> none  [body(): gathered = lax.all_gather(middle, ('kv', 'tp'), axis=1, tiled=True)]
    all_to_all x0 -> x1, blocking collectives: none -> 9.25 us  [body(): lax.all_to_all(jnp.stack([middle] * lax.axis_size(('kv', 'tp'))), ('kv',...]
    reduce_scatter x1, waiting for transfers between devices: 30.7 us -> 28.9 us  [body(): lax.psum_scatter(terms, ('kv', 'tp'), scatter_dimension=1, tiled=True)]
  transfers between devices with their start and end apart: 2 -> 2, of which waited for: 2 -> 2; matrix products, arithmetic and copies ran while one was open for 0% -> 1% of each run, Pallas kernels for 0% -> 0%
where the time goes in v1:
time: 130 us
  waiting for transfers between devices  65.2 us (50%)
  blocking collectives  25.6 us (20%)
  matrix products  16.4 us (13%)
  between operations  14.9 us (11%)
  other arithmetic  5.75 us (4%)
  local copies, waits for them, and re-layouts  1.74 us (1%)
    unnamed x3, waiting for transfers between devices  36.3 us
    reduce_scatter x1, waiting for transfers between devices, body(): lax.psum_scatter(terms, ('kv', 'tp'), scatter_dimension=1, tiled=True)  28.9 us
    all_gather x1, blocking collectives, body(): every_head = lax.all_gather(mixed, ('kv', 'tp'), axis=0, tiled=True)  14.1 us
    all_to_all x1, blocking collectives, body(): lax.all_to_all(jnp.stack([middle] * lax.axis_size(('kv', 'tp'))), ('kv',...  9.25 us
    dot_general x1, matrix products, body(): terms = jnp.dot(hidden, w_down, preferred_element_type=jnp.float32)  4.12 us
    dot_general x1, matrix products, body(): gate = jnp.dot(mlp_in, w_gate, preferred_element_type=jnp.float32)  2.66 us
  transfers between devices with their start and end apart: 2, of which 2 were waited for; matrix products, arithmetic and copies ran while one was open for 1% of the time, Pallas kernels for 0%

profile of v1, /device:TPU:0, one launch (start us, length us, event | category | flops | bytes accessed | tf_op | source)
XLA Modules:
  0.0 129.7 jit_solution(3326342565466569730)
XLA Ops:
  7.3 2.2 %all_gather.6 = bf16[8,512]{1,0:T(8,128)(2,1)S(1)} all-gather(bf16[8,256]{1,0:T(8,128)(2,1)} %param.14), channel_id=1, replica_groups=mesh['grp'=2,'dp'=2,'kv'=4,'tp'=2] {'tp'}, dimensions={1}, use_global_device_ids=true | all-gather | bytes 12288 | tf_op jit(solution)/shard_map/all_gather | solution.py:33
  9.5 0.6 fusion.10
  10.1 2.1 %fusion.31 = f32[8,1024]{1,0:T(8,128)} fusion(bf16[512,1024]{1,0:T(8,128)(2,1)} %param.19, bf16[8,512]{1,0:T(8,128)(2,1)S(1)} %all_gather.6, f32[512]{0:T(512)} %param.16), kind=kOutput, calls=%fused_computation.51 | convolution fusion | flops 8400896 | bytes 1091584 | tf_op jit(solution)/shard_map/dot_general | solution.py:53
  12.2 2.1 %fusion.29 = f32[8,1024]{1,0:T(8,128)} fusion(bf16[512,1024]{1,0:T(8,128)(2,1)} %param.17, bf16[8,512]{1,0:T(8,128)(2,1)S(1)} %all_gather.6, f32[512]{0:T(512)} %param.16), kind=kOutput, calls=%fused_computation.50 | convolution fusion | flops 8400896 | bytes 1091584 | tf_op jit(solution)/shard_map/dot_general | solution.py:41
  14.3 2.1 %fusion.27 = f32[8,1024]{1,0:T(8,128)} fusion(bf16[512,1024]{1,0:T(8,128)(2,1)} %param.20, bf16[8,512]{1,0:T(8,128)(2,1)S(1)} %all_gather.6, f32[512]{0:T(512)} %param.16), kind=kOutput, calls=%fused_computation.49 | convolution fusion | flops 8400896 | bytes 1091584 | tf_op jit(solution)/shard_map/dot_general | solution.py:59
  16.5 0.9 fusion.33
  17.4 0.0 reduce-scatter.2.cloned.1.call-start
  17.5 0.7 dynamic-slice
  18.8 36.2 %all-reduce.7.cloned.1.call-done = (f32[8,1024]{1,0:T(8,128)}, f32[8]{0:T(128)}, f32[8,1024]{1,0:T(8,128)}, f32[8,1024]{1,0:T(8,128)}, f32[8,1024]{1,0:T(8,128)}) async-done(((f32[8,1024]{1,0:T(8,128)}, f32[8]{0:T(128)}, f32[8,1024]{1,0:T(8,128)}, f32[8,1024]{1,0:T(8,128)}, f32[8,1024]{1,0:T(8,128)}), (f32[8,1024]{1,0:T(8,128)}, f32[8]{0:T(128)}, f32[8,1024]{1,0:T(8,128)}, f32[8,1024]{1,0:T(8,128)}, ...) | async-done | bytes 131120
  55.1 0.8 add_rsqrt_fusion.2
  55.8 0.9 fusion.21
  56.8 1.8 %multiply_add_fusion = f32[2,8,128,128]{3,2,1,0:T(8,128)S(1)} fusion(f32[2,8,128,128]{3,2,1,0:T(8,128)} %param.15, f32[2,8,128]{2,1,0:T(8,128)S(1)} %bitcast.84, f32[2,8,128]{2,1,0:T(8,128)S(1)} %get-tuple-element.7, f32[2,8,128]{2,1,0:T(8,128)S(1)} %get-tuple-element.8), kind=kLoop, calls=%fused_computation.6 | loop fusion | flops 786432 | bytes 2121728 | tf_op jit(solution)/shard_map/add | solution.py:72
  58.6 1.0 copy-done.1
  59.6 1.0 fusion.38
  60.6 0.1 multiply_reduce_fusion.1
  60.7 0.1 fusion.26
  60.8 14.1 %all_gather.7 = bf16[8,2,1024]{2,1,0:T(2,128)(2,1)S(1)} all-gather(bf16[1,2,1024]{2,1,0:T(2,128)(2,1)S(1)} %convert_element_type.56), channel_id=1, replica_groups=mesh['grp'=2,'dp'=2,'kv'=4,'tp'=2] {'kv','tp'}, dimensions={0}, use_global_device_ids=true | all-gather | bytes 36864 | tf_op jit(solution)/shard_map/all_gather | solution.py:78
  74.9 1.5 %fusion.3 = bf16[8,256]{1,0:T(8,128)(2,1)S(1)} fusion(bf16[8,1024,2]{1,0,2:T(8,128)(2,1)S(1)} %dot_general.37, bf16[2,1024,256]{2,1,0:T(8,128)(2,1)} %bitcast.78, bf16[8,256]{1,0:T(8,128)(2,1)S(1)} %copy-done.5), kind=kOutput, calls=%fused_computation.5 | convolution fusion | flops 8394752 | bytes 1089536 | tf_op jit(solution)/shard_map/ktsh,thc->ksc/dot_general | solution.py:81
  76.4 9.3 %all_to_all.5 = bf16[8,8,256]{2,1,0:T(8,128)(2,1)S(1)} all-to-all(bf16[8,8,256]{2,1,0:T(8,128)(2,1)S(1)} %stack.2), channel_id=1, replica_groups=mesh['grp'=2,'dp'=2,'kv'=4,'tp'=2] {'kv','tp'}, dimensions={0} | all-to-all | bytes 65536 | tf_op jit(solution)/shard_map/all_to_all | solution.py:88
  85.7 0.1 multiply_reduce_fusion
  85.8 2.7 %fusion.36 = f32[8,704]{1,0:T(8,128)S(1)} fusion(bf16[2048,704]{0,1:T(8,128)(2,1)} %param.25, f32[8,2048]{1,0:T(8,128)S(1)} %bitcast.79, f32[2048]{0:T(1024)S(1)} %copy-done.3, f32[8]{0:T(128)S(1)} %add_rsqrt_fusion.1), kind=kOutput, calls=%fused_computation.58 | convolution fusion | flops 23117824 | bytes 2979872 | tf_op jit(solution)/shard_map/dot_general | solution.py:94
  88.5 4.1 %fusion.1 = f32[8,2048]{1,0:T(8,128)} fusion(bf16[704,2048]{1,0:T(8,128)(2,1)S(1)} %copy-done, bf16[2048,704]{0,1:T(8,128)(2,1)} %param.26, f32[8,704]{1,0:T(8,128)S(1)} %fusion.36, f32[8,2048]{1,0:T(8,128)S(1)} %bitcast.80, f32[2048]{0:T(1024)S(1)} %copy-done.3, f32[8]{0:T(128)S(1)} %add_rsqrt_fusion.1), kind=kOutput, calls=%fused_computation.2 | convolution fusion | flops 46220288 | bytes 5928992 | tf_op jit(solution)/shard_map/dot_general | solution.py:97
  92.6 28.9 %reduce-scatter.2.cloned.1.call-done = f32[8,256]{1,0:T(8,128)} async-done(((f32[8,2048]{1,0:T(8,128)}), f32[8,256]{1,0:T(8,128)}) %reduce-scatter.2.cloned.1.call-update) | async-done | bytes 8208 | tf_op jit(solution)/shard_map/reduce_scatter | solution.py:98
  121.6 1.3 add_convert_fusion
  (31 shorter events, 0.2 us)
Async XLA Ops:
  7.2 81.3 %copy-start = (bf16[704,2048]{1,0:T(8,128)(2,1)S(1)}, bf16[704,2048]{1,0:T(8,128)(2,1)}, u32[]{:S(2)}) copy-start(bf16[704,2048]{1,0:T(8,128)(2,1)} %param.27) | copy-start | bytes 8650756
  7.2 10.3 %copy-start.8 = (u32[32]{0:T(128)S(1)}, u32[32]{0:T(128)}, u32[]{:S(2)}) copy-start(u32[32]{0:T(128)} %constant.38) | copy-start | bytes 388
  7.2 9.3 %copy-start.4 = (f32[512]{0:T(512)S(1)}, f32[512]{0:T(512)}, u32[]{:S(2)}) copy-start(f32[512]{0:T(512)} %param.16) | copy-start | bytes 6148
  7.2 10.2 %copy-start.6 = (f32[1024]{0:T(1024)S(1)}, f32[1024]{0:T(1024)}, u32[]{:S(2)}) copy-start(f32[1024]{0:T(1024)} %param.21) | copy-start | bytes 12292
  7.2 47.9 %all-reduce.7.cloned.1.call-start = ((), (), s32[]{:S(2)}) async-start(), calls=%async_computation.3 | async-start | bytes 263168
  7.3 9.2 %copy-start.2 = (bf16[512,1024]{1,0:T(8,128)(2,1)S(1)}, bf16[512,1024]{1,0:T(8,128)(2,1)}, u32[]{:S(2)}) copy-start(bf16[512,1024]{1,0:T(8,128)(2,1)} %param.18) | copy-start | bytes 3145732
  14.3 46.4 %copy-start.7 = (f32[128]{0:T(128)S(1)}, f32[128]{0:T(128)}, u32[]{:S(2)}) copy-start(f32[128]{0:T(128)} %param.22) | copy-start | bytes 1540
  14.3 60.6 %copy-start.5 = (bf16[8,256]{1,0:T(8,128)(2,1)S(1)}, bf16[8,256]{1,0:T(8,128)(2,1)}, u32[]{:S(2)}) copy-start(bf16[8,256]{1,0:T(8,128)(2,1)} %param.14) | copy-start | bytes 12292
  16.5 69.4 %copy-start.3 = (f32[2048]{0:T(1024)S(1)}, f32[2048]{0:T(1024)}, u32[]{:S(2)}) copy-start(f32[2048]{0:T(1024)} %param.24) | copy-start | bytes 24580
  17.4 104.2 %reduce-scatter.2.cloned.1.call-start = ((), (), s32[]{:S(2)}) async-start(), calls=%async_computation.2 | async-start | bytes 73728 | tf_op jit(solution)/shard_map/reduce_scatter | solution.py:98
  58.6 1.0 copy-start.1
Sparse Core Ops, SparseCore 0:
  17.5 37.5 all-reduce.6
  92.8 28.7 reduce-scatter.1
